TPU v7x, 512 devices: a whole 4x8x8 slice. The times are simulated.
512 devices in a mesh: sp: 128 (over z, y, core), tp: 4 (over x).
Axes of the slice: x: 4, y: 8, z: 8, core: 2. Of those that a mesh axis runs over, the one named last changes fastest.
Arguments:
- tokens: bfloat16 [32768, 2048], P(('sp', 'tp')), may hold values from -16 to 16
- w_query: bfloat16 [2048, 1024], P(None, 'tp'), may hold values from -1 to 1
- w_key: bfloat16 [2048, 256], P(None, 'tp'), may hold values from -1 to 1
- w_value: bfloat16 [2048, 256], P(None, 'tp'), may hold values from -0.125 to 0.125
- w_gate: bfloat16 [2048, 16], P(None, 'tp'), may hold values from -0.125 to 0.125
- gate_bias: float32 [16], P('tp'), as said below
- w_output: bfloat16 [1024, 2048], P('tp'), may hold values from -0.1875 to 0.1875
Outputs:
- mixed: bfloat16 [32768, 2048], P(('sp', 'tp'))
Inputs may be any that keep to these rules, and one draw needn't show every extreme that they name: `gate_bias`: each head's forget gate bias is 4 or more; there is no upper bound.
All inputs are finite; a program needn't handle non-finite values.
Results may differ from a plain program's by a relative error of at most 0.012.
The roundings to bfloat16 on the way count: a program that leaves them out, or rounds other values in their place, can miss the bound.
Values may be sent and summed in bfloat16 or wider, within the bound.
No kernel may reach another device: no remote copies, remote signals or barrier semaphores. Data moves between devices by JAX's collectives and lax.ppermute only.
A program may use at most 64 MiB of HBM per device.

v0:
```python
import math
import jax
import jax.numpy as jnp
from jax import lax
from jax.sharding import Mesh
from jax.sharding import PartitionSpec as P

HEAD = 64
SP = ("sp_0", "sp_1", "sp_2")
SP_TP = ("sp_0", "sp_1", "sp_2", "tp")
masked_value = -1e30


def copy_for_each(value, axis):
    copies = jnp.broadcast_to(value, (lax.axis_size(axis), *value.shape))
    return lax.all_to_all(copies, axis, split_axis=0, concat_axis=0, tiled=True)


def in_order(pieces, dim):
    lengths = list(pieces.shape[1:])
    lengths[dim] *= pieces.shape[0]
    return jnp.moveaxis(pieces, 0, dim).reshape(lengths)


def collect(value, axis, dim):
    pieces = copy_for_each(value, axis)
    return in_order(pieces, dim)


def all_blocks(value, axes, sequence):
    pieces = value
    for k in sequence:
        pieces = lax.all_gather(pieces, axes[k])
    done = sequence[::-1]
    back = [done.index(k) for k in range(len(axes))]
    pieces = pieces.transpose(*back, *range(len(axes), pieces.ndim))
    return pieces.reshape(-1, *value.shape)


def whole_of(value, axes, sequence, dim):
    return in_order(all_blocks(value, axes, sequence), dim)


def in_blocks(value, dim, count):
    lengths = value.shape
    pieces = value.reshape(*lengths[:dim], count, lengths[dim] // count, *lengths[dim + 1 :])
    return jnp.moveaxis(pieces, dim, 0)


def sum_at_owner(value, axis, dim):
    pieces = in_blocks(value, dim, lax.axis_size(axis))
    arrived = lax.all_to_all(pieces, axis, split_axis=0, concat_axis=0, tiled=True)
    return arrived.astype(jnp.float32).sum(axis=0)


def softmax_update(
    carry_state,
    query_here,
    query_cumul,
    query_position,
    key_here,
    value_here,
    key_cumul,
    key_position,
):
    row_peak, row_mass, row_accum = carry_state
    scores = jnp.einsum(
        "kgtd,skd->kgts", query_here, key_here, preferred_element_type=jnp.float32
    ) * HEAD ** (-0.5)
    scores = scores + query_cumul[:, :, :, None] - key_cumul[:, :, None, :]
    allowed = key_position[None, :] <= query_position[:, None]
    scores = jnp.where(allowed, scores, masked_value)
    new_peak = jnp.maximum(row_peak, jnp.max(scores, axis=3))
    weights = jnp.where(allowed, jnp.exp(scores - new_peak[:, :, :, None]), 0.0)
    rescale = jnp.exp(row_peak - new_peak)
    row_mass = row_mass * rescale + jnp.sum(weights, axis=3)
    row_accum = row_accum * rescale[:, :, :, None] + jnp.einsum(
        "kgts,skd->kgtd",
        weights.astype(jnp.bfloat16),
        value_here,
        preferred_element_type=jnp.float32,
    )
    return (new_peak, row_mass, row_accum)


def shards(tokens, w_query, w_key, w_value, w_gate, gate_bias, w_output):
    sp_count = lax.axis_size(SP)
    sp_rank = lax.axis_index(SP)
    query_cols = w_query.shape[1]
    key_cols = w_key.shape[1]
    heads_here = w_gate.shape[1]
    kv_heads_here = key_cols // HEAD
    group_size = heads_here // kv_heads_here
    joined = jnp.concatenate([w_query, w_key, w_value, w_gate], axis=1)
    projected = jnp.dot(
        collect(tokens, "tp", 0), joined, preferred_element_type=jnp.float32
    ).astype(jnp.bfloat16)
    local_rows = projected.shape[0]
    half_rows = local_rows // 2
    second_block = 2 * sp_rank + 1
    own_gates = jax.nn.log_sigmoid(
        projected[:, query_cols + 2 * key_cols :].astype(jnp.float32) + gate_bias
    )
    totals = jnp.sum(own_gates.reshape(2, half_rows, heads_here), axis=1)
    all_totals = whole_of(totals[None], (("sp_0", "sp_1"), "sp_2"), (0, 1), 0)
    ordered = all_totals.reshape(2 * sp_count, heads_here)
    prefix_sums = jnp.cumsum(ordered, axis=0) - ordered
    queries = (
        projected[:, :query_cols]
        .reshape(2, half_rows, kv_heads_here, group_size, HEAD)
        .transpose(0, 2, 3, 1, 4)
    )
    query_blocks = (2 * sp_rank, second_block)
    query_cumul = []
    query_position = []
    for side_index in range(2):
        base_value = lax.dynamic_index_in_dim(
            prefix_sums, query_blocks[side_index], 0, keepdims=False
        )
        cumul_rows = base_value[None, :] + jnp.cumsum(
            own_gates[side_index * half_rows : (side_index + 1) * half_rows], axis=0
        )
        query_cumul.append(
            cumul_rows.reshape(half_rows, kv_heads_here, group_size).transpose(1, 2, 0)
        )
        query_position.append(
            query_blocks[side_index] * half_rows + jnp.arange(half_rows, dtype=jnp.int32)
        )
    initial = (
        jnp.full((2, kv_heads_here, group_size, half_rows), masked_value, jnp.float32),
        jnp.zeros((2, kv_heads_here, group_size, half_rows), jnp.float32),
        jnp.zeros((2, kv_heads_here, group_size, half_rows, HEAD), jnp.float32),
    )
    gathered = lax.all_gather(projected[:, query_cols:], SP, axis=0, tiled=True)
    row_count = gathered.shape[0]
    piece_blocks = row_count // half_rows
    per_step = math.gcd(piece_blocks, max(1, 1024 // half_rows))
    step_rows = per_step * half_rows
    step_count = row_count // step_rows
    first_row = half_rows * jnp.arange(piece_blocks, dtype=jnp.int32)
    owner_rank = first_row // local_rows
    half_index = first_row % local_rows // half_rows
    block_ids = 2 * owner_rank + half_index
    gate_logs = jax.nn.log_sigmoid(gathered[:, 2 * key_cols :].astype(jnp.float32) + gate_bias)
    gate_logs = gate_logs.reshape(piece_blocks, half_rows, heads_here)
    base_values = jnp.take(prefix_sums, block_ids, axis=0)
    key_cumul_all = (base_values[:, None, :] + jnp.cumsum(gate_logs, axis=1)).reshape(
        row_count, kv_heads_here, group_size
    )
    key_position_all = (
        block_ids[:, None] * half_rows + jnp.arange(half_rows, dtype=jnp.int32)[None, :]
    ).reshape(row_count)
    earliest = jnp.min(block_ids.reshape(step_count, per_step), axis=1)

    def one_step(step_index, inner_state):
        start_row = step_index * step_rows
        block_rows = lax.dynamic_slice_in_dim(gathered, start_row, step_rows, 0)
        key_here = block_rows[:, :key_cols].reshape(step_rows, kv_heads_here, HEAD)
        value_here = block_rows[:, key_cols : 2 * key_cols].reshape(step_rows, kv_heads_here, HEAD)
        key_cumul = lax.dynamic_slice_in_dim(key_cumul_all, start_row, step_rows, 0).transpose(
            1, 2, 0
        )
        key_position = lax.dynamic_slice_in_dim(key_position_all, start_row, step_rows, 0)
        first_id = earliest[step_index]
        results = []
        for side_index in range(2):
            head_state = tuple((member[side_index] for member in inner_state))

            def compute(head_state, side_index=side_index):
                return softmax_update(
                    head_state,
                    queries[side_index],
                    query_cumul[side_index],
                    query_position[side_index],
                    key_here,
                    value_here,
                    key_cumul,
                    key_position,
                )

            head_state = lax.cond(
                first_id <= query_blocks[side_index],
                compute,
                lambda unchanged: unchanged,
                head_state,
            )
            results.append(head_state)
        return tuple((jnp.stack([results[0][member], results[1][member]]) for member in range(3)))

    row_peak, row_mass, row_accum = lax.fori_loop(0, step_count, one_step, initial)
    attended = (row_accum / row_mass[:, :, :, :, None]).astype(jnp.bfloat16)
    attended = attended.transpose(0, 3, 1, 2, 4).reshape(local_rows, heads_here * HEAD)
    mixed = sum_at_owner(
        jnp.dot(attended, w_output, preferred_element_type=jnp.float32).astype(jnp.bfloat16),
        "tp",
        0,
    )
    return mixed.astype(jnp.bfloat16)


def solution(mesh):
    finer = Mesh(mesh.devices.reshape(8, 8, 2, mesh.shape["tp"]), ("sp_0", "sp_1", "sp_2", "tp"))
    placed = (
        P(SP_TP, None),
        P(None, "tp"),
        P(None, "tp"),
        P(None, "tp"),
        P(None, "tp"),
        P("tp"),
        P("tp", None),
    )
    return jax.shard_map(
        shards, mesh=finer, in_specs=placed, out_specs=P(SP_TP, None), check_vma=False
    )
```

profile of v0, /device:TPU:504, one launch (start us, length us, event | category | flops | bytes accessed | tf_op | source)
XLA Modules:
  0.0 388.9 jit_solution(7107253783128811441)
XLA Ops:
  8.7 4.3 %all-to-all-start = ((bf16[4,64,2048]{2,1,0:T(8,128)(2,1)}), bf16[4,64,2048]{2,1,0:T(8,128)(2,1)S(1)}, u32[]{:S(2)}, u32[]{:S(2)}) async-start(bf16[4,64,2048]{2,1,0:T(8,128)(2,1)} %broadcast_in_dim.67), calls=%async_computation | async-start | bytes 2097152 | tf_op jit(solution)/shard_map/all_to_all | solution.py:16
  14.7 13.4 %all-to-all-done = bf16[4,64,2048]{2,1,0:T(8,128)(2,1)S(1)} async-done(((bf16[4,64,2048]{2,1,0:T(8,128)(2,1)}), bf16[4,64,2048]{2,1,0:T(8,128)(2,1)S(1)}, u32[]{:S(2)}, u32[]{:S(2)}) %all-to-all-start) | async-done | bytes 1048608 | tf_op jit(solution)/shard_map/all_to_all | solution.py:16
  28.1 2.5 fusion.47
  31.9 47.2 %all-gather.2 = f32[64,2,4]{2,1,0:T(2,128)S(1)} all-gather(f32[1,2,4]{2,1,0:T(2,128)S(1)} %bitcast.213), channel_id=2, replica_groups=mesh['sp_0'=8,'sp_1'=8,'sp_2'=2,'tp'=4] {'sp_0','sp_1'}, dimensions={0}, use_global_device_ids=true | all-gather | bytes 2080 | tf_op jit(solution)/shard_map/all_gather | solution.py:33
  84.7 35.0 %all-gather.5.cloned.1.call-done = bf16[32768,132]{0,1:T(8,128)(2,1)} async-done(((bf16[256,132]{0,1:T(8,128)(2,1)}), bf16[32768,132]{0,1:T(8,128)(2,1)}) %all-gather.5.cloned.1.call-update) | async-done | bytes 8650768 | tf_op jit(solution)/shard_map/all_gather | solution.py:134
  122.7 238.2 %while.18 = (s32[]{:T(128)}, f32[2,1,4,128]{3,2,1,0:T(4,128)S(1)}, f32[2,1,4,128]{3,2,1,0:T(4,128)S(1)}, f32[2,1,4,128,64]{3,4,2,1,0:T(8,128)S(1)}, s32[32]{0:T(...) while((s32[]{:T(128)}, f32[2,1,4,128]{3,2,1,0:T(4,128)S(1)}, ...), condition=%wide.region_16.17_spmd.clone, body=%wide.region_7.16_spmd.clone.sunk | while | flops 280433920 | bytes 16568903 | solution.py:190
  125.1 2.2 conditional.6
  127.9 2.2 conditional.7
  135.4 2.2 conditional.7
  140.0 2.2 conditional.6
  142.8 2.2 conditional.7
  147.4 2.2 conditional.6
  150.2 2.2 conditional.7
  154.8 2.2 conditional.6
  157.7 2.2 conditional.7
  162.3 2.2 conditional.6
  165.1 2.2 conditional.7
  169.7 2.2 conditional.6
  172.6 2.2 conditional.7
  177.2 2.2 conditional.6
  180.0 2.2 conditional.7
  187.5 2.2 conditional.7
  192.1 2.2 conditional.6
  194.9 2.2 conditional.7
  202.4 2.2 conditional.7
  207.0 2.2 conditional.6
  209.8 2.2 conditional.7
  217.2 2.2 conditional.7
  224.7 2.2 conditional.7
  232.1 2.2 conditional.7
  239.6 2.2 conditional.7
  247.0 2.2 conditional.7
  254.5 2.2 conditional.7
  261.9 2.2 conditional.7
  269.4 2.2 conditional.7
  276.8 2.2 conditional.7
  284.2 2.2 conditional.7
  291.7 2.2 conditional.7
  299.1 2.2 conditional.7
  306.6 2.2 conditional.7
  314.0 2.2 conditional.7
  321.5 2.2 conditional.7
  328.9 2.2 conditional.7
  336.4 2.2 conditional.7
  343.8 2.2 conditional.7
  351.2 2.2 conditional.7
  358.7 2.2 conditional.7
  361.6 19.5 %all_to_all.10 = bf16[4,64,2048]{2,1,0:T(8,128)(2,1)S(1)} all-to-all(bf16[4,64,2048]{2,1,0:T(8,128)(2,1)S(1)} %bitcast.197), channel_id=1, replica_groups=mesh['sp_0'=8,'sp_1'=8,'sp_2'=2,'tp'=4] {'tp'}, dimensions={0} | all-to-all | bytes 2097152 | tf_op jit(solution)/shard_map/all_to_all | solution.py:52
  (891 shorter events, 255.7 us)
Async XLA Ops:
  6.5 354.6 %copy-start = (bf16[256,2048]{1,0:T(8,128)(2,1)S(1)}, bf16[256,2048]{1,0:T(8,128)(2,1)}, u32[]{:S(2)}) copy-start(bf16[256,2048]{1,0:T(8,128)(2,1)} %param.19) | copy-start | bytes 3145732
  6.5 6.5 %copy-start.3 = (bf16[2048,4]{0,1:T(4,128)(2,1)S(1)}, bf16[2048,4]{0,1:T(4,128)(2,1)}, u32[]{:S(2)}) copy-start(bf16[2048,4]{0,1:T(4,128)(2,1)} %param.17) | copy-start | bytes 49156
  6.5 7.6 %copy-start.1 = (bf16[2048,64]{0,1:T(8,128)(2,1)S(1)}, bf16[2048,64]{0,1:T(8,128)(2,1)}, u32[]{:S(2)}) copy-start(bf16[2048,64]{0,1:T(8,128)(2,1)} %param.16) | copy-start | bytes 786436
  6.5 7.8 %copy-start.2 = (bf16[2048,64]{0,1:T(8,128)(2,1)S(1)}, bf16[2048,64]{0,1:T(8,128)(2,1)}, u32[]{:S(2)}) copy-start(bf16[2048,64]{0,1:T(8,128)(2,1)} %param.15) | copy-start | bytes 786436
  8.7 19.4 %all-to-all-start = ((bf16[4,64,2048]{2,1,0:T(8,128)(2,1)}), bf16[4,64,2048]{2,1,0:T(8,128)(2,1)S(1)}, u32[]{:S(2)}, u32[]{:S(2)}) async-start(bf16[4,64,2048]{2,1,0:T(8,128)(2,1)} %broadcast_in_dim.67), calls=%async_computation | async-start | bytes 2097152 | tf_op jit(solution)/shard_map/all_to_all | solution.py:16
  13.0 106.7 %all-gather.5.cloned.1.call-start = ((), (), s32[]{:S(2)}) async-start(), calls=%async_computation.2 | async-start | bytes 8982528 | tf_op jit(solution)/shard_map/all_gather | solution.py:134
  28.1 3.5 copy-start.4
Sparse Core Ops, SparseCore 0:
  31.4 88.1 all-gather.4
where the time goes:
time: 390 us; the launch traced here: 389 us
  matrix products  91.4 us (23%)
  blocking collectives  68.7 us (18%)
  local copies, waits for them, and re-layouts  59.3 us (15%)
  other arithmetic  55.4 us (14%)
  waiting for transfers between devices  48.4 us (12%)
  loops' own time  47.7 us (12%)
  between operations  13.7 us (4%)
  starting transfers between devices  4.29 us (1%)
    all_gather x2, blocking collectives, all_blocks(): pieces = lax.all_gather(pieces, axes[k])  49.1 us
    dot_general x64, matrix products, softmax_update(): jnp.einsum('kgtd,skd->kgts', query_here, key_here, preferred_element_type...  48.9 us
    another operation x1, loops' own time, shards(): lax.fori_loop(0, step_count, one_step, initial)  45.3 us
    dot_general x64, matrix products, softmax_update(): jnp.einsum('kgts,skd->kgtd', weights.astype(jnp.bfloat16), value_here, pr...  39.5 us
    reduce_sum x64, other arithmetic, softmax_update(): row_mass = row_mass * rescale + jnp.sum(weights, axis=3)  37.9 us
    all_gather x1, waiting for transfers between devices, shards(): gathered = lax.all_gather(projected[:, query_cols:], SP, axis=0, tiled=True)  35 us
    reshape x32, local copies, waits for them, and re-layouts, one_step(): block_rows[:, key_cols:2 * key_cols].reshape(step_rows, kv_heads_here, HEAD)  31.8 us
    all_to_all x1, blocking collectives, sum_at_owner(): lax.all_to_all(pieces, axis, split_axis=0, concat_axis=0, tiled=True)  19.5 us
  transfers between devices with their start and end apart: 2, of which 2 were waited for; matrix products, arithmetic and copies ran while one was open for 1% of the time, Pallas kernels for 0%

commit v1 on v0

--- a/solution.py
+++ b/solution.py
@@ -131,7 +131,9 @@
         jnp.zeros((2, kv_heads_here, group_size, half_rows), jnp.float32),
         jnp.zeros((2, kv_heads_here, group_size, half_rows, HEAD), jnp.float32),
     )
-    gathered = lax.all_gather(projected[:, query_cols:], SP, axis=0, tiled=True)
+    part = projected[:, query_cols:]
+    sent = jnp.stack([part] * lax.axis_size(SP))
+    gathered = jnp.concatenate(lax.all_to_all(sent, SP, 0, 0), axis=0)
     row_count = gathered.shape[0]
     piece_blocks = row_count // half_rows
     per_step = math.gcd(piece_blocks, max(1, 1024 // half_rows))

time: 390 us -> 633 us (1.62)
  blocking collectives: 68.7 us -> 312 us
  waiting for transfers between devices: 48.4 us -> 13.4 us
  local copies, waits for them, and re-layouts: 59.3 us -> 93.1 us
  between operations: 13.7 us -> 0.31 us
  starting transfers between devices: 4.29 us -> 16 us
    all_gather x2, blocking collectives: 49.1 us -> 294 us  [all_blocks(): pieces = lax.all_gather(pieces, axes[k])]
    all_gather x1 -> x0, waiting for transfers between devices: 35 us -> none  [shards(): gathered = lax.all_gather(projected[:, query_cols:], SP, axis=0, tiled=True)]
    unnamed x16 -> x20, local copies, waits for them, and re-layouts: 1.84 us -> 23.1 us
    all_to_all x0 -> x1, starting transfers between devices: none -> 11.6 us  [shards(): gathered = jnp.concatenate(lax.all_to_all(sent, SP, 0, 0), axis=0)]
    all_to_all x0 -> x1, local copies, waits for them, and re-layouts: none -> 9.04 us  [shards(): gathered = jnp.concatenate(lax.all_to_all(sent, SP, 0, 0), axis=0)]
  transfers between devices with their start and end apart: 2 -> 2, of which waited for: 2 -> 1; matrix products, arithmetic and copies ran while one was open for 1% -> 1% of each run, Pallas kernels for 0% -> 0%
where the time goes in v1:
time: 633 us; the launch traced here: 629 us
  blocking collectives  312 us (49%)
  local copies, waits for them, and re-layouts  93.1 us (15%)
  matrix products  91.5 us (14%)
  other arithmetic  55.4 us (9%)
  loops' own time  47.5 us (8%)
  starting transfers between devices  16 us (3%)
  waiting for transfers between devices  13.4 us (2%)
    all_gather x2, blocking collectives, all_blocks(): pieces = lax.all_gather(pieces, axes[k])  294 us
    dot_general x64, matrix products, softmax_update(): jnp.einsum('kgtd,skd->kgts', query_here, key_here, preferred_element_type...  49 us
    another operation x1, loops' own time, shards(): lax.fori_loop(0, step_count, one_step, initial)  45.4 us
    dot_general x64, matrix products, softmax_update(): jnp.einsum('kgts,skd->kgtd', weights.astype(jnp.bfloat16), value_here, pr...  39.5 us
    reduce_sum x64, other arithmetic, softmax_update(): row_mass = row_mass * rescale + jnp.sum(weights, axis=3)  37.9 us
    reshape x32, local copies, waits for them, and re-layouts, one_step(): block_rows[:, key_cols:2 * key_cols].reshape(step_rows, kv_heads_here, HEAD)  31.8 us
    unnamed x20, local copies, waits for them, and re-layouts  23.1 us
    dynamic_slice x32, local copies, waits for them, and re-layouts, one_step(): first_id = earliest[step_index]  18.8 us
  transfers between devices with their start and end apart: 2, of which 1 were waited for; matrix products, arithmetic and copies ran while one was open for 1% of the time, Pallas kernels for 0%

profile of v1, /device:TPU:504, one launch (start us, length us, event | category | flops | bytes accessed | tf_op | source)
XLA Modules:
  0.0 629.2 jit_solution(6939087339371117873)
XLA Ops:
  2.2 4.4 all-to-all-start
  8.3 13.4 %all-to-all-done = bf16[4,64,2048]{2,1,0:T(8,128)(2,1)S(1)} async-done(((bf16[4,64,2048]{2,1,0:T(8,128)(2,1)}), bf16[4,64,2048]{2,1,0:T(8,128)(2,1)S(1)}, u32[]{:S(2)}, u32[]{:S(2)}) %all-to-all-start) | async-done | bytes 1048608 | tf_op jit(solution)/shard_map/all_to_all | solution.py:16
  21.7 2.5 fusion.47
  24.3 4.0 stack.92
  28.3 11.6 %all-to-all-start.1 = ((bf16[128,256,132]{1,2,0:T(8,128)(2,1)}), bf16[128,256,132]{1,2,0:T(8,128)(2,1)}, u32[]{:S(2)}, u32[]{:S(2)}) async-start(bf16[128,256,132]{1,2,0:T(8,128)(2,1)} %stack.92), calls=%async_computation.1 | async-start | bytes 17825792 | tf_op jit(solution)/shard_map/all_to_all | solution.py:136
  40.5 291.7 %all-gather.2 = f32[64,2,4]{2,1,0:T(2,128)S(1)} all-gather(f32[1,2,4]{2,1,0:T(2,128)S(1)} %bitcast.224), channel_id=2, replica_groups=mesh['sp_0'=8,'sp_1'=8,'sp_2'=2,'tp'=4] {'sp_0','sp_1'}, dimensions={0}, use_global_device_ids=true | all-gather | bytes 2080 | tf_op jit(solution)/shard_map/all_gather | solution.py:33
  338.0 9.0 %copy.110 = bf16[128,256,132]{1,0,2:T(8,128)(2,1)} copy(bf16[128,256,132]{1,2,0:T(8,128)(2,1)} %all-to-all-done.1) | data formatting | bytes 17301504 | tf_op jit(solution)/shard_map/all_to_all | solution.py:136
  347.0 8.1 %pad.11 = bf16[136,128,256]{2,1,0:T(8,128)(2,1)} pad(bf16[132,128,256]{2,1,0:T(8,128)(2,1)} %bitcast.203, bf16[]{:T(256)} %constant.166.clone.1), padding=0_4x0_0x0_0 | pad | bytes 17563650
  355.1 13.1 %copy.100 = bf16[17,8,128,256]{3,1,2,0:T(8,128)(2,1)} copy(bf16[17,8,128,256]{3,2,1,0:T(8,128)(2,1)} %bitcast.202) | data formatting | bytes 17825792
  371.3 238.2 %while.18 = (s32[]{:T(128)}, f32[2,1,4,128]{3,2,1,0:T(4,128)S(1)}, f32[2,1,4,128]{3,2,1,0:T(4,128)S(1)}, f32[2,1,4,128,64]{3,4,2,1,0:T(8,128)S(1)}, s32[32]{0:T(...) while((s32[]{:T(128)}, f32[2,1,4,128]{3,2,1,0:T(4,128)S(1)}, ...), condition=%wide.region_16.17_spmd.clone, body=%wide.region_7.16_spmd.clone.sunk | while | flops 280433920 | bytes 16568895 | solution.py:192
  373.9 2.2 conditional.7
  381.3 2.2 conditional.7
  388.7 2.2 conditional.7
  391.6 2.2 conditional.6
  396.2 2.2 conditional.7
  399.0 2.2 conditional.6
  403.6 2.2 conditional.7
  406.5 2.2 conditional.6
  411.1 2.2 conditional.7
  413.9 2.2 conditional.6
  418.5 2.2 conditional.7
  421.3 2.2 conditional.6
  425.9 2.2 conditional.7
  433.4 2.2 conditional.7
  440.8 2.2 conditional.7
  448.2 2.2 conditional.7
  455.7 2.2 conditional.7
  463.1 2.2 conditional.7
  470.5 2.2 conditional.7
  478.0 2.2 conditional.7
  485.4 2.2 conditional.7
  492.8 2.2 conditional.7
  500.3 2.2 conditional.7
  507.7 2.2 conditional.7
  515.2 2.2 conditional.7
  522.6 2.2 conditional.7
  530.0 2.2 conditional.7
  537.5 2.2 conditional.7
  544.9 2.2 conditional.7
  552.3 2.2 conditional.7
  559.8 2.2 conditional.7
  567.2 2.2 conditional.7
  574.6 2.2 conditional.7
  582.1 2.2 conditional.7
  589.5 2.2 conditional.7
  596.9 2.2 conditional.7
  604.4 2.2 conditional.7
  610.1 18.1 %all_to_all.15 = bf16[4,64,2048]{2,1,0:T(8,128)(2,1)S(1)} all-to-all(bf16[4,64,2048]{2,1,0:T(8,128)(2,1)S(1)} %bitcast.208), channel_id=1, replica_groups=mesh['sp_0'=8,'sp_1'=8,'sp_2'=2,'tp'=4] {'tp'}, dimensions={0} | all-to-all | bytes 2097152 | tf_op jit(solution)/shard_map/all_to_all | solution.py:52
  (897 shorter events, 264.1 us)
Async XLA Ops:
  0.0 609.7 %copy-start = (bf16[256,2048]{1,0:T(8,128)(2,1)S(1)}, bf16[256,2048]{1,0:T(8,128)(2,1)}, u32[]{:S(2)}) copy-start(bf16[256,2048]{1,0:T(8,128)(2,1)} %param.19) | copy-start | bytes 3145732
  0.0 6.6 %copy-start.2 = (bf16[2048,64]{0,1:T(8,128)(2,1)S(1)}, bf16[2048,64]{0,1:T(8,128)(2,1)}, u32[]{:S(2)}) copy-start(bf16[2048,64]{0,1:T(8,128)(2,1)} %param.15) | copy-start | bytes 786436
  0.0 6.9 %copy-start.3 = (bf16[2048,64]{0,1:T(8,128)(2,1)S(1)}, bf16[2048,64]{0,1:T(8,128)(2,1)}, u32[]{:S(2)}) copy-start(bf16[2048,64]{0,1:T(8,128)(2,1)} %param.16) | copy-start | bytes 786436
  2.2 5.0 copy-start.4
  2.2 19.5 %all-to-all-start = ((bf16[4,64,2048]{2,1,0:T(8,128)(2,1)}), bf16[4,64,2048]{2,1,0:T(8,128)(2,1)S(1)}, u32[]{:S(2)}, u32[]{:S(2)}) async-start(bf16[4,64,2048]{2,1,0:T(8,128)(2,1)} %broadcast_in_dim.67), calls=%async_computation | async-start | bytes 2097152 | tf_op jit(solution)/shard_map/all_to_all | solution.py:16
  24.2 15.9 %copy-start.1 = (bf16[256,388]{0,1:T(8,128)(2,1)}, bf16[256,388]{0,1:T(8,128)(2,1)S(1)}, u32[]{:S(2)}) copy-start(bf16[256,388]{0,1:T(8,128)(2,1)S(1)} %fusion.47) | copy-start | bytes 595972
  28.3 11.9 %copy-start.5 = (f32[4]{0:T(128)S(1)}, f32[4]{0:T(128)}, u32[]{:S(2)}) copy-start(f32[4]{0:T(128)} %param.18) | copy-start | bytes 52
  28.3 309.7 %all-to-all-start.1 = ((bf16[128,256,132]{1,2,0:T(8,128)(2,1)}), bf16[128,256,132]{1,2,0:T(8,128)(2,1)}, u32[]{:S(2)}, u32[]{:S(2)}) async-start(bf16[128,256,132]{1,2,0:T(8,128)(2,1)} %stack.92), calls=%async_computation.1 | async-start | bytes 17825792 | tf_op jit(solution)/shard_map/all_to_all | solution.py:136
  40.3 297.6 %slice-start = ((bf16[256,388]{0,1:T(8,128)(2,1)}), bf16[256,256]{0,1:T(8,128)(2,1)S(1)}, s32[]{:S(2)}) async-start(bf16[256,388]{0,1:T(8,128)(2,1)} %copy-done.1), calls=%async_computation.3 | async-start | bytes 262144 | tf_op jit(solution)/shard_map/slice | solution.py:109
